TPU v7x, 32 devices: a whole 2x2x4 slice. The times are simulated.
32 devices in a mesh: fs: 16 (over z, y, x), tp: 2 (over core).
Axes of the slice: x: 2, y: 2, z: 4, core: 2. Of those that a mesh axis runs over, the one named last changes fastest.
Arguments:
- inputs: bfloat16 [6144, 2048], P('fs'), may hold values from -6 to 6
- gain: float32 [2048], replicated, may hold values from 0.1 to 1.9
- w_gate: bfloat16 [2048, 2816], P('fs', 'tp'), may hold values from -0.125 to 0.125
- w_up: bfloat16 [2048, 2816], P('fs', 'tp'), may hold values from -0.125 to 0.125
- w_down: bfloat16 [2816, 2048], P('tp', 'fs'), may hold values from -0.109375 to 0.109375
- cotangent: bfloat16 [6144, 2048], P('fs'), may hold values from -6 to 6
Outputs:
- input_gradient: bfloat16 [6144, 2048], P('fs')
- grad_down: float32 [2816, 2048], P('tp', 'fs')
All inputs are finite; a program needn't handle non-finite values.
Results may differ from a plain program's by a relative error of at most 0.014.
Values may be sent and summed in bfloat16 or wider, within the bound.
A program may use at most 64 MiB of HBM per device.

v0:
```python
import jax
import jax.numpy as jnp
from jax import lax
from jax.sharding import PartitionSpec as P

EPSILON = 1e-06
HALF_STEP = 0.5


def contract_last(left, right):
    return lax.dot_general(
        left, right, (((1,), (1,)), ((), ())), preferred_element_type=jnp.float32
    )


def shards(inputs, gain, w_gate, w_up, w_down, cotangent):
    value_entries = inputs.astype(jnp.float32)
    inverse_norm_factor = lax.rsqrt(
        jnp.mean(value_entries * value_entries, axis=-1, keepdims=True) + EPSILON
    )
    normalized_input = value_entries * inverse_norm_factor
    normalized_rows = (normalized_input * gain).astype(jnp.bfloat16)
    whole_gate, whole_up = (
        lax.all_gather(w_gate, "fs", axis=0, tiled=True),
        lax.all_gather(w_up, "fs", axis=0, tiled=True),
    )
    gate_value = jnp.dot(normalized_rows, whole_gate, preferred_element_type=jnp.float32)
    up_projection_value = jnp.dot(normalized_rows, whole_up, preferred_element_type=jnp.float32)
    sigmoid_gate = jax.nn.sigmoid(gate_value)
    hidden = (gate_value * sigmoid_gate * up_projection_value).astype(jnp.bfloat16)
    d_hidden = HALF_STEP * contract_last(
        cotangent, lax.all_gather(w_down, "fs", axis=1, tiled=True)
    )
    down_term = HALF_STEP * lax.dot_general(
        hidden, cotangent, (((0,), (0,)), ((), ())), preferred_element_type=jnp.float32
    )
    grad_down = lax.psum_scatter(down_term, "fs", scatter_dimension=1, tiled=True)
    d_gate = (
        d_hidden * up_projection_value * sigmoid_gate * (1.0 + gate_value * (1.0 - sigmoid_gate))
    ).astype(jnp.bfloat16)
    d_up = (d_hidden * gate_value * sigmoid_gate).astype(jnp.bfloat16)
    partial_term = contract_last(d_gate, whole_gate) + contract_last(d_up, whole_up)
    d_normed = lax.psum(partial_term.astype(jnp.bfloat16), "tp").astype(jnp.float32)
    scaled_hidden = d_normed * gain
    input_gradient = inverse_norm_factor * (
        scaled_hidden
        - normalized_input * jnp.mean(scaled_hidden * normalized_input, axis=-1, keepdims=True)
    )
    return (input_gradient.astype(jnp.bfloat16), grad_down)


def solution(mesh):
    in_specs = (P("fs", None), P(), P("fs", "tp"), P("fs", "tp"), P("tp", "fs"), P("fs", None))
    out_specs = (P("fs", None), P("tp", "fs"))
    return jax.shard_map(shards, mesh=mesh, in_specs=in_specs, out_specs=out_specs, check_vma=False)
```

profile of v0, /device:TPU:10, one launch (start us, length us, event | category | flops | bytes accessed | tf_op | source)
XLA Modules:
  0.0 587.9 jit_solution(5369307967862374800)
XLA Ops:
  7.2 0.0 all-gather.8.cloned.1.call-start
  7.2 0.7 all-gather.8.cloned.1.call-update
  7.9 0.0 all-gather.6.cloned.1.call-start
  8.0 0.7 all-gather.6.cloned.1.call-update
  8.7 0.0 all-gather.4.cloned.1.call-start
  8.7 0.7 all-gather.4.cloned.1.call-update
  9.4 0.0 all-reduce.2.cloned.1.call-start
  9.5 1.8 fusion.8
  11.3 89.2 %all-gather.8.cloned.1.call-done = bf16[2048,1408]{1,0:T(8,128)(2,1)} async-done(((bf16[128,1408]{1,0:T(8,128)(2,1)}), bf16[2048,1408]{1,0:T(8,128)(2,1)}) %all-gather.8.cloned.1.call-update) | async-done | bytes 5767184 | tf_op jit(solution)/shard_map/all_gather | solution.py:24
  100.5 6.6 %fusion.13 = f32[384,1408]{1,0:T(8,128)} fusion(bf16[2048,1408]{1,0:T(8,128)(2,1)} %all-gather.8.cloned.1.call-done, bf16[384,2048]{1,0:T(8,128)(2,1)S(1)} %copy-done.1, f32[2048]{0:T(1024)S(1)} %copy-done.3, f32[384]{0:T(512)S(1)} %add_rsqrt_fusion), kind=kOutput, calls=%fused_computation.23 | convolution fusion | flops 2217738240 | bytes 9512448 | tf_op jit(solution)/shard_map/dot_general | solution.py:27
  107.1 83.5 %all-gather.6.cloned.1.call-done = bf16[2048,1408]{1,0:T(8,128)(2,1)} async-done(((bf16[128,1408]{1,0:T(8,128)(2,1)}), bf16[2048,1408]{1,0:T(8,128)(2,1)}) %all-gather.6.cloned.1.call-update) | async-done | bytes 5767184 | tf_op jit(solution)/shard_map/all_gather | solution.py:25
  190.6 6.7 %fusion.15 = f32[384,1408]{1,0:T(8,128)} fusion(bf16[2048,1408]{1,0:T(8,128)(2,1)} %all-gather.6.cloned.1.call-done, bf16[384,2048]{1,0:T(8,128)(2,1)S(1)} %copy-done.1, f32[2048]{0:T(1024)S(1)} %copy-done.3, f32[384]{0:T(512)S(1)} %add_rsqrt_fusion), kind=kOutput, calls=%fused_computation.24 | convolution fusion | flops 2217738240 | bytes 9512448 | tf_op jit(solution)/shard_map/dot_general | solution.py:28
  197.3 100.4 %all-gather.4.cloned.1.call-done = bf16[1408,2048]{1,0:T(8,128)(2,1)} async-done(((bf16[1408,128]{1,0:T(8,128)(2,1)}), bf16[1408,2048]{1,0:T(8,128)(2,1)}) %all-gather.4.cloned.1.call-update) | async-done | bytes 5767184 | tf_op jit(solution)/shard_map/all_gather | solution.py:32
  297.7 5.4 convolution_multiply_fusion.1
  303.2 0.1 copy-done.6
  303.3 3.2 fusion.9
  306.6 3.8 add_convert_fusion
  310.4 0.0 all-reduce.2.cloned.1.call-update
  310.4 0.2 reduce-scatter.2.cloned.1.call-start
  310.6 8.5 %convolution_multiply_fusion = f32[1408,2048]{1,0:T(8,128)} fusion(bf16[384,2048]{1,0:T(8,128)(2,1)S(1)} %copy-done, f32[384,1408]{1,0:T(8,128)} %fusion.15, f32[384,1408]{1,0:T(8,128)} %fusion.13), kind=kOutput, calls=%fused_computation | convolution fusion | flops 2220720128 | bytes 17432576 | tf_op jit(solution)/shard_map/dot_general | solution.py:34
  319.1 13.0 %all-reduce.2.cloned.1.call-done = bf16[384,2048]{1,0:T(8,128)(2,1)} async-done(((bf16[384,2048]{1,0:T(8,128)(2,1)}), bf16[384,2048]{1,0:T(8,128)(2,1)}) %all-reduce.2.cloned.1.call-update) | async-done | bytes 1572880 | tf_op jit(solution)/shard_map/psum | solution.py:43
  332.1 2.3 fusion.4
  334.4 2.0 fusion.7
  336.5 245.0 %reduce-scatter.2.cloned.1.call-done = f32[1408,128]{1,0:T(8,128)} async-done(((f32[1408,2048]{1,0:T(8,128)}), f32[1408,128]{1,0:T(8,128)}) %reduce-scatter.2.cloned.1.call-update) | async-done | bytes 720912 | tf_op jit(solution)/shard_map/reduce_scatter | solution.py:37
  (21 shorter events, 0.1 us)
Async XLA Ops:
  7.2 290.6 %copy-start = (bf16[384,2048]{1,0:T(8,128)(2,1)S(1)}, bf16[384,2048]{1,0:T(8,128)(2,1)}, u32[]{:S(2)}) copy-start(bf16[384,2048]{1,0:T(8,128)(2,1)} %param.11) | copy-start | bytes 4718596
  7.2 93.3 %copy-start.1 = (bf16[384,2048]{1,0:T(8,128)(2,1)S(1)}, bf16[384,2048]{1,0:T(8,128)(2,1)}, u32[]{:S(2)}) copy-start(bf16[384,2048]{1,0:T(8,128)(2,1)} %param.6) | copy-start | bytes 4718596
  7.2 93.3 %copy-start.3 = (f32[2048]{0:T(1024)S(1)}, f32[2048]{0:T(1024)}, u32[]{:S(2)}) copy-start(f32[2048]{0:T(1024)} %param.7) | copy-start | bytes 24580
  7.2 93.3 %all-gather.8.cloned.1.call-start = ((), (), s32[]{:S(2)}) async-start(), calls=%async_computation.3 | async-start | bytes 6127616 | tf_op jit(solution)/shard_map/all_gather | solution.py:24
  7.9 182.7 %all-gather.6.cloned.1.call-start = ((), (), s32[]{:S(2)}) async-start(), calls=%async_computation.2 | async-start | bytes 6127616 | tf_op jit(solution)/shard_map/all_gather | solution.py:25
  8.7 289.0 %all-gather.4.cloned.1.call-start = ((), (), s32[]{:S(2)}) async-start(), calls=%async_computation.1 | async-start | bytes 6127616 | tf_op jit(solution)/shard_map/all_gather | solution.py:32
  9.4 322.7 %all-reduce.2.cloned.1.call-start = ((), (), s32[]{:S(2)}) async-start(), calls=%async_computation.4 | async-start | bytes 3145728 | tf_op jit(solution)/shard_map/psum | solution.py:43
  297.7 5.4 copy-start.4
  297.7 5.5 copy-start.5
  297.7 5.6 copy-start.6
  297.7 8.8 %slice-start = ((s8[5767168]{0:T(1024)(128)(4,1)}), s8[4194304]{0:T(1024)(128)(4,1)S(1)}, s32[]{:S(2)}) async-start(s8[5767168]{0:T(1024)(128)(4,1)} %bitcast.7), calls=%async_computation.6 | async-start | bytes 8388608
  303.3 3.2 slice-start.1
  310.4 271.0 %reduce-scatter.2.cloned.1.call-start = ((), (), s32[]{:S(2)}) async-start(), calls=%async_computation.5 | async-start | bytes 12255232 | tf_op jit(solution)/shard_map/reduce_scatter | solution.py:37
  332.1 2.3 copy-start.2
Sparse Core Ops, SparseCore 0:
  10.7 89.7 all-gather.7
  103.2 87.4 all-gather.5
  193.3 104.3 all-gather.3
  310.5 21.5 all-reduce.1
  334.9 246.5 reduce-scatter.1
where the time goes:
time: 588 us
  waiting for transfers between devices  533 us (91%)
  matrix products  34.2 us (6%)
  between operations  13.9 us (2%)
  other arithmetic  6.11 us (1%)
    reduce_scatter x1, waiting for transfers between devices, shards(): lax.psum_scatter(down_term, 'fs', scatter_dimension=1, tiled=True)  245 us
    all_gather x1, waiting for transfers between devices, shards(): lax.all_gather(w_down, 'fs', axis=1, tiled=True)  100 us
    all_gather x1, waiting for transfers between devices, shards(): lax.all_gather(w_gate, 'fs', axis=0, tiled=True)  89.2 us
    all_gather x1, waiting for transfers between devices, shards(): lax.all_gather(w_up, 'fs', axis=0, tiled=True)  83.5 us
    psum x1, waiting for transfers between devices, shards(): lax.psum(partial_term.astype(jnp.bfloat16), 'tp').astype(jnp.float32)  13 us
    dot_general x3, matrix products, contract_last(): lax.dot_general(left, right, (((1,), (1,)), ((), ())), preferred_element_...  12.4 us
  transfers between devices with their start and end apart: 5, of which 5 were waited for; matrix products, arithmetic and copies ran while one was open for 5% of the time, Pallas kernels for 0%

commit v1 on v0

--- a/solution.py
+++ b/solution.py
@@ -1,7 +1,12 @@
+import functools
+
 import jax
 import jax.numpy as jnp
 from jax import lax
+from jax.experimental import pallas as pl
+from jax.experimental.pallas import tpu as pltpu
 from jax.sharding import PartitionSpec as P
+
 
 EPSILON = 1e-06
 HALF_STEP = 0.5
@@ -49,7 +54,272 @@
     return (input_gradient.astype(jnp.bfloat16), grad_down)
 
 
+RING = 4
+MESH_ID = pl.DeviceIdType.MESH
+
+
+def gray(i):
+    return i + (i // 2) * (1 - 2 * (i % 2))
+
+
+def branch_kernel(
+    x_ref, n_ref, c_ref, gain_ref, wp_ref, ig_ref, gd_ref,
+    tok_n, tok_c, wt, dn, dpart, rs, gd_acc, gd_send, gd_rs, gd_sum,
+    s_wa, r_wa, s_wz, r_wz, s_wr, r_wr, s_t, r_t, s_tr, r_tr, s_dd, r_dd,
+    s_dn, r_dn, s_rs, r_rs, s_gz, r_gz, s_gp, r_gp, s_ig, r_ig,
+):
+    fs = lax.axis_index("fs")
+    tp = lax.axis_index("tp")
+    zi = fs // RING
+    pi = fs % RING
+    ring = gray(pi)
+    rows = n_ref.shape[0]
+    half = rows // 2
+    hq = wp_ref.shape[2]
+    dl = wp_ref.shape[3]
+    partner = (fs, 1 - tp)
+    mine = pl.ds(pl.multiple_of(tp * half, half), half)
+    other = pl.ds(pl.multiple_of((1 - tp) * half, half), half)
+
+    def plane_fs(k, dz=0):
+        return ((zi + dz) % 4) * RING + gray((ring + k) % RING)
+
+    def cols(f, width=dl):
+        return pl.ds(pl.multiple_of(f * width, width), width)
+
+    def copy(src, dst, ssem, rsem, dev):
+        return pltpu.make_async_remote_copy(
+            src_ref=src, dst_ref=dst, send_sem=ssem, recv_sem=rsem,
+            device_id=dev, device_id_type=MESH_ID,
+        )
+
+    pending = []
+
+    def send(src, dst, ssem, rsem, dev):
+        c = copy(src, dst, ssem, rsem, dev)
+        c.start()
+        pending.append(c)
+
+    def arrived(dst, ssem, rsem, dev):
+        copy(dst, dst, ssem, rsem, dev).wait_recv()
+
+    barrier = pltpu.get_barrier_semaphore()
+    peers = [partner] + [(plane_fs(k), tp) for k in (1, 2, 3)] + [(plane_fs(0, k), tp) for k in (1, 2, 3)]
+    for peer in peers:
+        pl.semaphore_signal(barrier, inc=1, device_id=peer, device_id_type=MESH_ID)
+    pl.semaphore_wait(barrier, len(peers))
+
+    for k in (1, 3, 2):
+        f = plane_fs(k)
+        send(wp_ref.at[f % RING], wt.at[:, :, cols(fs)], s_wa.at[k - 1], r_wa.at[k - 1], (f, tp))
+    for d, dz in ((0, 1), (1, -1)):
+        send(wp_ref.at[pi], wt.at[:, :, cols(fs)], s_wz.at[d, 0], r_wz.at[d, 0], (plane_fs(0, dz), tp))
+    for t, src, buf in ((0, n_ref, tok_n), (1, c_ref, tok_c)):
+        for d, k in ((0, 1), (1, 3)):
+            send(src.at[mine, :], buf.at[4 - k, mine, :], s_t.at[t, d], r_t.at[t, d], (plane_fs(k), tp))
+    tok_n[0] = n_ref[...]
+    tok_c[0] = c_ref[...]
+    wt[:, :, cols(fs)] = wp_ref[pi]
+    gd_acc[...] = jnp.zeros_like(gd_acc)
+
+    for k in (1, 3, 2):
+        s = 4 - k
+        place = wt.at[:, :, cols(plane_fs(s))]
+        arrived(place, s_wa.at[k - 1], r_wa.at[k - 1], (plane_fs(s), tp))
+        for d, dz in ((0, 1), (1, -1)):
+            send(place, place, s_wz.at[d, s], r_wz.at[d, s], (plane_fs(0, dz), tp))
+    for s in (0, 3, 1, 2):
+        for d, dz in ((0, -1), (1, 1)):
+            place = wt.at[:, :, cols(plane_fs(s, dz))]
+            arrived(place, s_wz.at[d, s], r_wz.at[d, s], (plane_fs(0, dz), tp))
+            if s % 2 == d:
+                send(place, place, s_wr.at[s], r_wr.at[s], (plane_fs(0, -dz), tp))
+
+    def to_partner(t, buf, slot):
+        place = buf.at[slot, mine, :]
+        send(place, place, s_dd.at[t, slot], r_dd.at[t, slot], partner)
+
+    for t, buf in ((0, tok_n), (1, tok_c)):
+        for d, slot in ((0, 3), (1, 1)):
+            place = buf.at[slot, mine, :]
+            arrived(place, s_t.at[t, d], r_t.at[t, d], (plane_fs(slot), tp))
+            if t == d:
+                send(place, buf.at[2, mine, :], s_tr.at[t], r_tr.at[t], (plane_fs(4 - slot), tp))
+            to_partner(t, buf, slot)
+    for s in (0, 3, 1, 2):
+        place = wt.at[:, :, cols(plane_fs(s, 2))]
+        arrived(place, s_wr.at[s], r_wr.at[s], (plane_fs(0, 1), tp))
+
+    def exchange(b):
+        return copy(dn.at[b, other, :], dpart.at[b], s_dn.at[b], r_dn.at[b], partner)
+
+    def rs_copy(b):
+        return copy(dn.at[b, mine, :], rs.at[b], s_rs.at[b], r_rs.at[b], (plane_fs(b), tp))
+
+    def chip_sum(b):
+        exchange(b).wait_recv()
+        dn[b, mine, :] = (
+            dn[b, mine, :].astype(jnp.float32) + dpart[b].astype(jnp.float32)
+        ).astype(jnp.bfloat16)
+
+    def last_tokens():
+        for t, buf in ((0, tok_n), (1, tok_c)):
+            place = buf.at[2, mine, :]
+            arrived(place, s_tr.at[t], r_tr.at[t], (plane_fs(1), tp))
+            copy(place, place, s_dd.at[t, 2], r_dd.at[t, 2], partner).start()
+
+    def step(i, carry):
+        b = gray(i)
+        pl.when(i == 3)(last_tokens)
+
+        @pl.when(i > 0)
+        def _():
+            for t, buf in ((0, tok_n), (1, tok_c)):
+                place = buf.at[b, other, :]
+                arrived(place, s_dd.at[t, b], r_dd.at[t, b], partner)
+
+        n_b = tok_n[b]
+        c_b = tok_c[b]
+        gate = contract_last(n_b, wt[0])
+        up = contract_last(n_b, wt[1])
+        d_hidden = HALF_STEP * contract_last(c_b, wt[2])
+        sig = jax.nn.sigmoid(gate)
+        act = gate * sig
+        hidden = (act * up).astype(jnp.bfloat16)
+        d_gate = (d_hidden * up * sig * (1.0 + gate * (1.0 - sig))).astype(jnp.bfloat16)
+        d_up = (d_hidden * act).astype(jnp.bfloat16)
+        dn[b] = (
+            jnp.dot(d_gate, wt[0], preferred_element_type=jnp.float32)
+            + jnp.dot(d_up, wt[1], preferred_element_type=jnp.float32)
+        ).astype(jnp.bfloat16)
+        exchange(b).start()
+        gd_acc[...] += lax.dot_general(
+            hidden, c_b, (((0,), (0,)), ((), ())), preferred_element_type=jnp.float32
+        )
+
+        @pl.when(i >= 2)
+        def _():
+            last = gray(i - 1)
+            chip_sum(last)
+            rs_copy(last).start()
+
+        return carry
+
+    lax.fori_loop(0, 4, step, 0)
+
+    gd_send[...] = (HALF_STEP * gd_acc[...]).astype(jnp.bfloat16)
+    wide = RING * dl
+    gz = [
+        copy(gd_send.at[:, cols((zi + k) % 4, wide)], gd_rs.at[k - 1], s_gz.at[k - 1], r_gz.at[k - 1], (plane_fs(0, k), tp))
+        for k in (1, 2, 3)
+    ]
+    for c in (gz[1], gz[0], gz[2]):
+        c.start()
+    chip_sum(2)
+    rs_copy(2).start()
+    chip_sum(0)
+    for c in gz:
+        c.wait_recv()
+    total = HALF_STEP * gd_acc[:, cols(zi, wide)]
+    for k in range(3):
+        total = total + gd_rs[k].astype(jnp.float32)
+    for q in range(RING):
+        gd_sum[q] = total[:, q * dl:(q + 1) * dl]
+    here = pl.ds(pl.multiple_of(pi * hq, hq), hq)
+    for k in (1, 3, 2):
+        f = plane_fs(k)
+        send(gd_sum.at[f % RING], gd_ref.at[here, :], s_gp.at[k - 1], r_gp.at[k - 1], (f, tp))
+    gd_ref[here, :] = gd_sum[pi]
+
+    for b in (1, 3, 2):
+        rs_copy(b).wait_recv()
+    d_normed = dn[0, mine, :].astype(jnp.float32)
+    for b in (1, 2, 3):
+        d_normed = d_normed + rs[b].astype(jnp.float32)
+    values = x_ref[mine, :].astype(jnp.float32)
+    inverse = lax.rsqrt(jnp.mean(values * values, axis=-1, keepdims=True) + EPSILON)
+    xhat = values * inverse
+    scaled = d_normed * gain_ref[...]
+    ig_ref[mine, :] = (
+        inverse * (scaled - xhat * jnp.mean(scaled * xhat, axis=-1, keepdims=True))
+    ).astype(jnp.bfloat16)
+    final = copy(ig_ref.at[mine, :], ig_ref.at[mine, :], s_ig, r_ig, partner)
+    final.start()
+
+    for k in (1, 3, 2):
+        there = pl.ds(pl.multiple_of((plane_fs(4 - k) % RING) * hq, hq), hq)
+        arrived(gd_ref.at[there, :], s_gp.at[k - 1], r_gp.at[k - 1], (plane_fs(4 - k), tp))
+    arrived(ig_ref.at[other, :], s_ig, r_ig, partner)
+    final.wait_send()
+    for c in pending + gz:
+        c.wait_send()
+    for t, buf in ((0, tok_n), (1, tok_c)):
+        place = buf.at[2, mine, :]
+        copy(place, place, s_dd.at[t, 2], r_dd.at[t, 2], partner).wait_send()
+    for b in range(RING):
+        exchange(b).wait_send()
+        if b:
+            rs_copy(b).wait_send()
+
+
+def fused(inputs, gain, w_gate, w_up, w_down, cotangent):
+    rows, d = inputs.shape
+    dl, hl = w_gate.shape
+    hq = hl // RING
+    values = inputs.astype(jnp.float32)
+    inverse = lax.rsqrt(jnp.mean(values * values, axis=-1, keepdims=True) + EPSILON)
+    normed = (values * inverse * gain).astype(jnp.bfloat16)
+
+    def turned(w):
+        return w.reshape(dl, RING, hq).transpose(1, 2, 0)
+
+    packed = jnp.stack([turned(w_gate), turned(w_up), w_down.reshape(RING, hq, dl)], axis=1)
+    half = rows // 2
+    bf, f32 = jnp.bfloat16, jnp.float32
+    dma = pltpu.SemaphoreType.DMA
+    vm = pl.BlockSpec(memory_space=pltpu.VMEM)
+    pairs = [(3,), (2, 4), (4,), (2, 2), (2,), (2, 4), (4,), (4,), (3,), (3,)]
+    sems = []
+    for p in pairs:
+        sems += [dma(p), dma(p)]
+    sems += [dma, dma]
+    return pl.pallas_call(
+        branch_kernel,
+        out_shape=(jax.ShapeDtypeStruct((rows, d), bf), jax.ShapeDtypeStruct((hl, dl), f32)),
+        in_specs=[vm] * 5,
+        out_specs=(vm, vm),
+        scratch_shapes=[
+            pltpu.VMEM((RING, rows, d), bf),
+            pltpu.VMEM((RING, rows, d), bf),
+            pltpu.VMEM((3, hq, d), bf),
+            pltpu.VMEM((RING, rows, d), bf),
+            pltpu.VMEM((RING, half, d), bf),
+            pltpu.VMEM((RING, half, d), bf),
+            pltpu.VMEM((hq, d), f32),
+            pltpu.VMEM((hq, d), bf),
+            pltpu.VMEM((3, hq, RING * dl), bf),
+            pltpu.VMEM((RING, hq, dl), f32),
+        ] + sems,
+        compiler_params=pltpu.CompilerParams(
+            collective_id=0, has_side_effects=True, vmem_limit_bytes=67043328
+        ),
+    )(inputs, normed, cotangent, gain.reshape(1, d), packed)
+
+
+def fits(mesh, w_gate_shape, rows):
+    n_fs, n_tp = mesh.shape["fs"], mesh.shape["tp"]
+    dl, hl = w_gate_shape[0] // n_fs, w_gate_shape[1] // n_tp
+    return n_fs == RING * RING and n_tp == 2 and dl % 128 == 0 and hl % (16 * RING) == 0 and rows // n_fs % 32 == 0
+
+
 def solution(mesh):
     in_specs = (P("fs", None), P(), P("fs", "tp"), P("fs", "tp"), P("tp", "fs"), P("fs", None))
     out_specs = (P("fs", None), P("tp", "fs"))
-    return jax.shard_map(shards, mesh=mesh, in_specs=in_specs, out_specs=out_specs, check_vma=False)
+
+    def run(inputs, gain, w_gate, w_up, w_down, cotangent):
+        body = fused if fits(mesh, w_gate.shape, inputs.shape[0]) else shards
+        return jax.shard_map(
+            body, mesh=mesh, in_specs=in_specs, out_specs=out_specs, check_vma=False
+        )(inputs, gain, w_gate, w_up, w_down, cotangent)
+
+    return run

time: 588 us -> 157 us (0.27)
  waiting for transfers between devices: 533 us -> 0 us
  Pallas kernels: 0 us -> 146 us
  matrix products: 34.2 us -> 0 us
  between operations: 13.9 us -> 0.72 us
    all_gather x3 -> x0, waiting for transfers between devices: 273 us -> none  [the longest x1 100 us: shards(): lax.all_gather(w_down, 'fs', axis=1, tiled=True)]
    reduce_scatter x1 -> x0, waiting for transfers between devices: 245 us -> none  [shards(): lax.psum_scatter(down_term, 'fs', scatter_dimension=1, tiled=True)]
    pallas_call x0 -> x1, Pallas kernels: none -> 146 us  [fused(): pl.pallas_call(branch_kernel, out_shape=(jax.ShapeDtypeStruct((rows, d),...]
    dot_general x6 -> x0, matrix products: 34.2 us -> none  [the longest x3 12.4 us: contract_last(): lax.dot_general(left, right, (((1,), (1,)), ((), ())), preferred_element_...]
    psum x1 -> x0, waiting for transfers between devices: 13 us -> none  [shards(): lax.psum(partial_term.astype(jnp.bfloat16), 'tp').astype(jnp.float32)]
  transfers between devices with their start and end apart: 5 -> 0, of which waited for: 5 -> 0; matrix products, arithmetic and copies ran while one was open for 5% -> 0% of each run, Pallas kernels for 0% -> 0%
where the time goes in v1:
time: 157 us; the launch traced here: 156 us
  Pallas kernels  146 us (93%)
  other arithmetic  4.56 us (3%)
  local copies, waits for them, and re-layouts  4.32 us (3%)
    pallas_call x1, Pallas kernels, fused(): pl.pallas_call(branch_kernel, out_shape=(jax.ShapeDtypeStruct((rows, d),...  146 us
    unnamed x16, local copies, waits for them, and re-layouts  4.32 us

profile of v1, /device:TPU:10, one launch (start us, length us, event | category | flops | bytes accessed | tf_op | source)
XLA Modules:
  0.0 155.9 jit_solution(8354918099631547057)
XLA Ops:
  0.6 0.0 copy-start.4
  0.6 0.0 copy-start.3
  0.7 0.0 copy-start.2
  0.7 1.9 %fusion = f32[384]{0:T(512)S(1)} fusion(bf16[384,2048]{1,0:T(8,128)(2,1)} %x_ref.1), kind=kLoop, calls=%fused_computation.2 | loop fusion | flops 2358912 | bytes 1574400 | tf_op jit(solution)/shard_map/reduce_sum | solution.py:270
  2.5 0.0 copy-done.2
  2.6 0.2 copy.8
  2.8 0.0 copy-start
  2.8 0.0 copy-start.5
  2.8 0.0 copy-done.3
  2.8 0.2 copy.9
  3.0 0.0 copy-done.4
  3.1 1.1 pad_maximum_fusion.wp_ref
  4.2 0.2 copy-done
  4.4 0.0 copy-done.5
  4.4 1.6 %fusion.2.n_ref = bf16[384,2048]{1,0:T(8,128)(2,1)} fusion(bf16[384,2048]{1,0:T(8,128)(2,1)S(1)} %copy-done, f32[2048]{0:T(1024)S(1)} %copy-done.5, f32[384]{0:T(512)S(1)} %add_rsqrt_fusion), kind=kLoop, calls=%fused_computation.4 | loop fusion | flops 3145728 | bytes 3155456 | tf_op jit(solution)/shard_map/convert_element_type | solution.py:271
  5.9 146.3 %shard_map.77 = (bf16[384,2048]{1,0:T(8,128)(2,1)}, f32[1408,128]{1,0:T(8,128)}) custom-call(bf16[384,2048]{1,0:T(8,128)(2,1)} %x_ref.1, bf16[384,2048]{1,0:T(8,128)(2,1)} %fusion.2.n_ref, bf16[384,2048]{1,0:T(8,128)(2,1)} %c_ref.1, f32[1,2048]{1,0:T(1,128)} %bitcast.15, bf16[4,3,352,128]{3,2,1,0:T(8,128)(2,1)} %pad_maximum_fusion.wp_ref), custom_call_target="tpu_custom_call" | custom-call | tf_op jit(solution)/shard_map/pallas_call | solution.py:286
  152.2 0.0 copy-start.1
  152.3 2.8 %copy.12 = bf16[384,2048]{1,0:T(8,128)(2,1)} copy(bf16[384,2048]{1,0:T(8,128)(2,1)} %get-tuple-element.4) | data formatting | bytes 3145728
  155.1 0.0 copy-done.1
  155.1 0.9 copy.13
  (1 shorter events, 0.0 us)
Async XLA Ops:
  0.6 2.4 %copy-start.4 = (bf16[1408,128]{1,0:T(8,128)(2,1)S(1)}, bf16[1408,128]{1,0:T(8,128)(2,1)}, u32[]{:S(2)}) copy-start(bf16[1408,128]{1,0:T(8,128)(2,1)} %param.10) | copy-start | bytes 1081348
  0.6 2.2 %copy-start.3 = (bf16[128,1408]{1,0:T(8,128)(2,1)S(1)}, bf16[128,1408]{1,0:T(8,128)(2,1)}, u32[]{:S(2)}) copy-start(bf16[128,1408]{1,0:T(8,128)(2,1)} %param.9) | copy-start | bytes 1081348
  0.7 1.9 %copy-start.2 = (bf16[128,1408]{1,0:T(8,128)(2,1)S(1)}, bf16[128,1408]{1,0:T(8,128)(2,1)}, u32[]{:S(2)}) copy-start(bf16[128,1408]{1,0:T(8,128)(2,1)} %param.8) | copy-start | bytes 1081348
  2.8 1.6 %copy-start = (bf16[384,2048]{1,0:T(8,128)(2,1)S(1)}, bf16[384,2048]{1,0:T(8,128)(2,1)}, u32[]{:S(2)}) copy-start(bf16[384,2048]{1,0:T(8,128)(2,1)} %x_ref.1) | copy-start | bytes 4718596
  2.8 1.6 %copy-start.5 = (f32[2048]{0:T(1024)S(1)}, f32[2048]{0:T(1024)}, u32[]{:S(2)}) copy-start(f32[2048]{0:T(1024)} %param.7) | copy-start | bytes 24580
  152.2 2.8 %copy-start.1 = (f32[1408,128]{1,0:T(8,128)S(1)}, f32[1408,128]{1,0:T(8,128)}, u32[]{:S(2)}) copy-start(f32[1408,128]{1,0:T(8,128)} %get-tuple-element.5) | copy-start | bytes 2162692

commit v2 on v1

--- a/solution.py
+++ b/solution.py
@@ -64,22 +64,24 @@
 
 def branch_kernel(
     x_ref, n_ref, c_ref, gain_ref, wp_ref, ig_ref, gd_ref,
-    tok_n, tok_c, wt, dn, dpart, rs, gd_acc, gd_send, gd_rs, gd_sum,
+    tok_n, tok_c, wt, dn, dpart, rs, r_opp, slope, act, gd_acc, gd_send, gd_rs, gd_sum,
     s_wa, r_wa, s_wz, r_wz, s_wr, r_wr, s_t, r_t, s_tr, r_tr, s_dd, r_dd,
-    s_dn, r_dn, s_rs, r_rs, s_gz, r_gz, s_gp, r_gp, s_ig, r_ig,
+    s_dn, r_dn, s_rs, r_rs, s_op, r_op, s_gz, r_gz, s_gp, r_gp, s_ig, r_ig,
 ):
     fs = lax.axis_index("fs")
     tp = lax.axis_index("tp")
     zi = fs // RING
     pi = fs % RING
     ring = gray(pi)
-    rows = n_ref.shape[0]
+    rows, width_d = n_ref.shape
     half = rows // 2
     hq = wp_ref.shape[2]
     dl = wp_ref.shape[3]
     partner = (fs, 1 - tp)
     mine = pl.ds(pl.multiple_of(tp * half, half), half)
     other = pl.ds(pl.multiple_of((1 - tp) * half, half), half)
+    low, high = pl.ds(0, width_d // 2), pl.ds(width_d // 2, width_d // 2)
+    parts = (pl.ds(0, 2), pl.ds(2, 1))
 
     def plane_fs(k, dz=0):
         return ((zi + dz) % 4) * RING + gray((ring + k) % RING)
@@ -109,66 +111,83 @@
         pl.semaphore_signal(barrier, inc=1, device_id=peer, device_id_type=MESH_ID)
     pl.semaphore_wait(barrier, len(peers))
 
-    for k in (1, 3, 2):
-        f = plane_fs(k)
-        send(wp_ref.at[f % RING], wt.at[:, :, cols(fs)], s_wa.at[k - 1], r_wa.at[k - 1], (f, tp))
-    for d, dz in ((0, 1), (1, -1)):
-        send(wp_ref.at[pi], wt.at[:, :, cols(fs)], s_wz.at[d, 0], r_wz.at[d, 0], (plane_fs(0, dz), tp))
-    for t, src, buf in ((0, n_ref, tok_n), (1, c_ref, tok_c)):
+    def weights_plane(p):
+        for k in (1, 3, 2):
+            f = plane_fs(k)
+            send(
+                wp_ref.at[f % RING, parts[p]], wt.at[parts[p], :, cols(fs)],
+                s_wa.at[p, k - 1], r_wa.at[p, k - 1], (f, tp),
+            )
+
+    def weights_own(p):
+        for d, dz in ((0, 1), (1, -1)):
+            send(
+                wp_ref.at[pi, parts[p]], wt.at[parts[p], :, cols(fs)],
+                s_wz.at[p, d, 0], r_wz.at[p, d, 0], (plane_fs(0, dz), tp),
+            )
+
+    def weights_forward(p):
+        for k in (1, 3, 2):
+            s = 4 - k
+            place = wt.at[parts[p], :, cols(plane_fs(s))]
+            arrived(place, s_wa.at[p, k - 1], r_wa.at[p, k - 1], (plane_fs(s), tp))
+            for d, dz in ((0, 1), (1, -1)):
+                send(place, place, s_wz.at[p, d, s], r_wz.at[p, d, s], (plane_fs(0, dz), tp))
+
+    def relay(p, s, d, dz):
+        place = wt.at[parts[p], :, cols(plane_fs(s, dz))]
+        return copy(place, place, s_wr.at[p, s], r_wr.at[p, s], (plane_fs(0, -dz), tp))
+
+    def weights_relay(p):
+        for s in (0, 3, 1, 2):
+            for d, dz in ((0, -1), (1, 1)):
+                place = wt.at[parts[p], :, cols(plane_fs(s, dz))]
+                arrived(place, s_wz.at[p, d, s], r_wz.at[p, d, s], (plane_fs(0, dz), tp))
+                if s % 2 == d:
+                    relay(p, s, d, dz).start()
+
+    def weights_last(p):
+        for s in (0, 3, 1, 2):
+            place = wt.at[parts[p], :, cols(plane_fs(s, 2))]
+            arrived(place, s_wr.at[p, s], r_wr.at[p, s], (plane_fs(0, 1), tp))
+
+    def tokens_own(t, src, buf):
         for d, k in ((0, 1), (1, 3)):
             send(src.at[mine, :], buf.at[4 - k, mine, :], s_t.at[t, d], r_t.at[t, d], (plane_fs(k), tp))
-    tok_n[0] = n_ref[...]
-    tok_c[0] = c_ref[...]
-    wt[:, :, cols(fs)] = wp_ref[pi]
-    gd_acc[...] = jnp.zeros_like(gd_acc)
-
-    for k in (1, 3, 2):
-        s = 4 - k
-        place = wt.at[:, :, cols(plane_fs(s))]
-        arrived(place, s_wa.at[k - 1], r_wa.at[k - 1], (plane_fs(s), tp))
-        for d, dz in ((0, 1), (1, -1)):
-            send(place, place, s_wz.at[d, s], r_wz.at[d, s], (plane_fs(0, dz), tp))
-    for s in (0, 3, 1, 2):
-        for d, dz in ((0, -1), (1, 1)):
-            place = wt.at[:, :, cols(plane_fs(s, dz))]
-            arrived(place, s_wz.at[d, s], r_wz.at[d, s], (plane_fs(0, dz), tp))
-            if s % 2 == d:
-                send(place, place, s_wr.at[s], r_wr.at[s], (plane_fs(0, -dz), tp))
-
-    def to_partner(t, buf, slot):
-        place = buf.at[slot, mine, :]
-        send(place, place, s_dd.at[t, slot], r_dd.at[t, slot], partner)
-
-    for t, buf in ((0, tok_n), (1, tok_c)):
+
+    def tokens_relay(t, buf):
         for d, slot in ((0, 3), (1, 1)):
             place = buf.at[slot, mine, :]
             arrived(place, s_t.at[t, d], r_t.at[t, d], (plane_fs(slot), tp))
             if t == d:
                 send(place, buf.at[2, mine, :], s_tr.at[t], r_tr.at[t], (plane_fs(4 - slot), tp))
-            to_partner(t, buf, slot)
-    for s in (0, 3, 1, 2):
-        place = wt.at[:, :, cols(plane_fs(s, 2))]
-        arrived(place, s_wr.at[s], r_wr.at[s], (plane_fs(0, 1), tp))
-
-    def exchange(b):
-        return copy(dn.at[b, other, :], dpart.at[b], s_dn.at[b], r_dn.at[b], partner)
-
-    def rs_copy(b):
-        return copy(dn.at[b, mine, :], rs.at[b], s_rs.at[b], r_rs.at[b], (plane_fs(b), tp))
-
-    def chip_sum(b):
-        exchange(b).wait_recv()
-        dn[b, mine, :] = (
-            dn[b, mine, :].astype(jnp.float32) + dpart[b].astype(jnp.float32)
-        ).astype(jnp.bfloat16)
+            send(place, place, s_dd.at[t, slot], r_dd.at[t, slot], partner)
+
+    weights_plane(0)
+    weights_own(0)
+    tokens_own(0, n_ref, tok_n)
+    weights_plane(1)
+    tokens_own(1, c_ref, tok_c)
+    tok_n[0] = n_ref[...]
+    tok_c[0] = c_ref[...]
+    wt[:, :, cols(fs)] = wp_ref[pi]
+    gd_acc[...] = jnp.zeros_like(gd_acc)
+    weights_forward(0)
+    tokens_relay(0, tok_n)
+    weights_relay(0)
+    weights_own(1)
+    weights_forward(1)
+    tokens_relay(1, tok_c)
+    weights_last(0)
 
     def last_tokens():
+        weights_relay(1)
         for t, buf in ((0, tok_n), (1, tok_c)):
             place = buf.at[2, mine, :]
             arrived(place, s_tr.at[t], r_tr.at[t], (plane_fs(1), tp))
             copy(place, place, s_dd.at[t, 2], r_dd.at[t, 2], partner).start()
 
-    def step(i, carry):
+    def forward(i, carry):
         b = gray(i)
         pl.when(i == 3)(last_tokens)
 
@@ -179,33 +198,19 @@
                 arrived(place, s_dd.at[t, b], r_dd.at[t, b], partner)
 
         n_b = tok_n[b]
-        c_b = tok_c[b]
         gate = contract_last(n_b, wt[0])
         up = contract_last(n_b, wt[1])
-        d_hidden = HALF_STEP * contract_last(c_b, wt[2])
         sig = jax.nn.sigmoid(gate)
-        act = gate * sig
-        hidden = (act * up).astype(jnp.bfloat16)
-        d_gate = (d_hidden * up * sig * (1.0 + gate * (1.0 - sig))).astype(jnp.bfloat16)
-        d_up = (d_hidden * act).astype(jnp.bfloat16)
-        dn[b] = (
-            jnp.dot(d_gate, wt[0], preferred_element_type=jnp.float32)
-            + jnp.dot(d_up, wt[1], preferred_element_type=jnp.float32)
-        ).astype(jnp.bfloat16)
-        exchange(b).start()
+        gated = gate * sig
+        hidden = (gated * up).astype(jnp.bfloat16)
+        slope[b] = up * sig * (1.0 + gate * (1.0 - sig))
+        act[b] = gated
         gd_acc[...] += lax.dot_general(
-            hidden, c_b, (((0,), (0,)), ((), ())), preferred_element_type=jnp.float32
+            hidden, tok_c[b], (((0,), (0,)), ((), ())), preferred_element_type=jnp.float32
         )
-
-        @pl.when(i >= 2)
-        def _():
-            last = gray(i - 1)
-            chip_sum(last)
-            rs_copy(last).start()
-
         return carry
 
-    lax.fori_loop(0, 4, step, 0)
+    lax.fori_loop(0, 4, forward, 0)
 
     gd_send[...] = (HALF_STEP * gd_acc[...]).astype(jnp.bfloat16)
     wide = RING * dl
@@ -215,8 +220,65 @@
     ]
     for c in (gz[1], gz[0], gz[2]):
         c.start()
-    chip_sum(2)
-    rs_copy(2).start()
+    weights_last(1)
+
+    def exchange(b):
+        return copy(dn.at[b, other, :], dpart.at[b], s_dn.at[b], r_dn.at[b], partner)
+
+    def rs_copy(b, part):
+        place = (low, high)[part]
+        e = 0 if b == 1 else 1
+        return copy(dn.at[b, mine, place], rs.at[e, :, place], s_rs.at[e, part], r_rs.at[e, part], (plane_fs(b), tp))
+
+    def opp_copy(e):
+        return copy(
+            dn.at[2, mine, (low, high)[e]], r_opp.at[e],
+            s_op.at[e], r_op.at[e], (plane_fs((1, 3)[e]), tp),
+        )
+
+    def chip_sum(b):
+        exchange(b).wait_recv()
+        dn[b, mine, :] = (
+            dn[b, mine, :].astype(jnp.float32) + dpart[b].astype(jnp.float32)
+        ).astype(jnp.bfloat16)
+
+    def backward(i, carry):
+        b = jnp.where(i == 0, 2, jnp.where(i == 3, 0, 2 * i - 1))
+        d_hidden = HALF_STEP * contract_last(tok_c[b], wt[2])
+        d_gate = (d_hidden * slope[b]).astype(jnp.bfloat16)
+        d_up = (d_hidden * act[b]).astype(jnp.bfloat16)
+        dn[b] = (
+            jnp.dot(d_gate, wt[0], preferred_element_type=jnp.float32)
+            + jnp.dot(d_up, wt[1], preferred_element_type=jnp.float32)
+        ).astype(jnp.bfloat16)
+        exchange(b).start()
+
+        @pl.when(i == 1)
+        def _():
+            chip_sum(2)
+            opp_copy(0).start()
+            opp_copy(1).start()
+
+        @pl.when(i == 2)
+        def _():
+            chip_sum(1)
+            rs_copy(1, 1).start()
+
+        @pl.when(i == 3)
+        def _():
+            chip_sum(3)
+            rs_copy(3, 0).start()
+
+        return carry
+
+    lax.fori_loop(0, 4, backward, 0)
+
+    for e, b, place in ((0, 1, low), (1, 3, high)):
+        opp_copy(e).wait_recv()
+        dn[b, mine, place] = (
+            dn[b, mine, place].astype(jnp.float32) + r_opp[e].astype(jnp.float32)
+        ).astype(jnp.bfloat16)
+        rs_copy(b, e).start()
     chip_sum(0)
     for c in gz:
         c.wait_recv()
@@ -231,11 +293,12 @@
         send(gd_sum.at[f % RING], gd_ref.at[here, :], s_gp.at[k - 1], r_gp.at[k - 1], (f, tp))
     gd_ref[here, :] = gd_sum[pi]
 
-    for b in (1, 3, 2):
-        rs_copy(b).wait_recv()
+    for b in (1, 3):
+        for part in (0, 1):
+            rs_copy(b, part).wait_recv()
     d_normed = dn[0, mine, :].astype(jnp.float32)
-    for b in (1, 2, 3):
-        d_normed = d_normed + rs[b].astype(jnp.float32)
+    for e in (0, 1):
+        d_normed = d_normed + rs[e].astype(jnp.float32)
     values = x_ref[mine, :].astype(jnp.float32)
     inverse = lax.rsqrt(jnp.mean(values * values, axis=-1, keepdims=True) + EPSILON)
     xhat = values * inverse
@@ -253,13 +316,18 @@
     final.wait_send()
     for c in pending + gz:
         c.wait_send()
+    for p in (0, 1):
+        for s in range(RING):
+            relay(p, s, s % 2, (-1, 1)[s % 2]).wait_send()
     for t, buf in ((0, tok_n), (1, tok_c)):
         place = buf.at[2, mine, :]
         copy(place, place, s_dd.at[t, 2], r_dd.at[t, 2], partner).wait_send()
     for b in range(RING):
         exchange(b).wait_send()
-        if b:
-            rs_copy(b).wait_send()
+    for e in (0, 1):
+        opp_copy(e).wait_send()
+        for part in (0, 1):
+            rs_copy((1, 3)[e], part).wait_send()
 
 
 def fused(inputs, gain, w_gate, w_up, w_down, cotangent):
@@ -278,7 +346,7 @@
     bf, f32 = jnp.bfloat16, jnp.float32
     dma = pltpu.SemaphoreType.DMA
     vm = pl.BlockSpec(memory_space=pltpu.VMEM)
-    pairs = [(3,), (2, 4), (4,), (2, 2), (2,), (2, 4), (4,), (4,), (3,), (3,)]
+    pairs = [(2, 3), (2, 2, 4), (2, 4), (2, 2), (2,), (2, 4), (4,), (2, 2), (2,), (3,), (3,)]
     sems = []
     for p in pairs:
         sems += [dma(p), dma(p)]
@@ -294,7 +362,10 @@
             pltpu.VMEM((3, hq, d), bf),
             pltpu.VMEM((RING, rows, d), bf),
             pltpu.VMEM((RING, half, d), bf),
-            pltpu.VMEM((RING, half, d), bf),
+            pltpu.VMEM((2, half, d), bf),
+            pltpu.VMEM((2, half, d // 2), bf),
+            pltpu.VMEM((RING, rows, hq), f32),
+            pltpu.VMEM((RING, rows, hq), f32),
             pltpu.VMEM((hq, d), f32),
             pltpu.VMEM((hq, d), bf),
             pltpu.VMEM((3, hq, RING * dl), bf),

time: 157 us -> 133 us (0.85)
  the two profiles are of different devices: /device:TPU:10 before, /device:TPU:0 now
where the time goes in v2:
time: 133 us
  Pallas kernels  123 us (92%)
  other arithmetic  4.56 us (3%)
  local copies, waits for them, and re-layouts  4.32 us (3%)
    pallas_call x1, Pallas kernels, fused(): pl.pallas_call(branch_kernel, out_shape=(jax.ShapeDtypeStruct((rows, d),...  123 us
    unnamed x16, local copies, waits for them, and re-layouts  4.32 us

profile of v2, /device:TPU:0, one launch (start us, length us, event | category | flops | bytes accessed | tf_op | source)
XLA Modules:
  0.0 133.0 jit_solution(5930143844141419729)
XLA Ops:
  0.6 0.0 copy-start.4
  0.6 0.0 copy-start.3
  0.7 0.0 copy-start.2
  0.7 1.9 %fusion = f32[384]{0:T(512)S(1)} fusion(bf16[384,2048]{1,0:T(8,128)(2,1)} %x_ref.1), kind=kLoop, calls=%fused_computation.2 | loop fusion | flops 2358912 | bytes 1574400 | tf_op jit(solution)/shard_map/reduce_sum | solution.py:338
  2.5 0.0 copy-done.2
  2.6 0.2 copy.8
  2.8 0.0 copy-start
  2.8 0.0 copy-start.5
  2.8 0.0 copy-done.3
  2.8 0.2 copy.9
  3.0 0.0 copy-done.4
  3.1 1.1 pad_maximum_fusion.wp_ref
  4.2 0.2 copy-done
  4.4 0.0 copy-done.5
  4.4 1.6 %fusion.2.n_ref = bf16[384,2048]{1,0:T(8,128)(2,1)} fusion(bf16[384,2048]{1,0:T(8,128)(2,1)S(1)} %copy-done, f32[2048]{0:T(1024)S(1)} %copy-done.5, f32[384]{0:T(512)S(1)} %add_rsqrt_fusion), kind=kLoop, calls=%fused_computation.4 | loop fusion | flops 3145728 | bytes 3155456 | tf_op jit(solution)/shard_map/convert_element_type | solution.py:339
  5.9 123.4 %shard_map.77 = (bf16[384,2048]{1,0:T(8,128)(2,1)}, f32[1408,128]{1,0:T(8,128)}) custom-call(bf16[384,2048]{1,0:T(8,128)(2,1)} %x_ref.1, bf16[384,2048]{1,0:T(8,128)(2,1)} %fusion.2.n_ref, bf16[384,2048]{1,0:T(8,128)(2,1)} %c_ref.1, f32[1,2048]{1,0:T(1,128)} %bitcast.15, bf16[4,3,352,128]{3,2,1,0:T(8,128)(2,1)} %pad_maximum_fusion.wp_ref), custom_call_target="tpu_custom_call" | custom-call | tf_op jit(solution)/shard_map/pallas_call | solution.py:354
  129.4 0.0 copy-start.1
  129.4 2.8 %copy.12 = bf16[384,2048]{1,0:T(8,128)(2,1)} copy(bf16[384,2048]{1,0:T(8,128)(2,1)} %get-tuple-element.4) | data formatting | bytes 3145728
  132.2 0.0 copy-done.1
  132.2 0.9 copy.13
  (1 shorter events, 0.0 us)
Async XLA Ops:
  0.6 2.4 %copy-start.4 = (bf16[1408,128]{1,0:T(8,128)(2,1)S(1)}, bf16[1408,128]{1,0:T(8,128)(2,1)}, u32[]{:S(2)}) copy-start(bf16[1408,128]{1,0:T(8,128)(2,1)} %param.10) | copy-start | bytes 1081348
  0.6 2.2 %copy-start.3 = (bf16[128,1408]{1,0:T(8,128)(2,1)S(1)}, bf16[128,1408]{1,0:T(8,128)(2,1)}, u32[]{:S(2)}) copy-start(bf16[128,1408]{1,0:T(8,128)(2,1)} %param.9) | copy-start | bytes 1081348
  0.7 1.9 %copy-start.2 = (bf16[128,1408]{1,0:T(8,128)(2,1)S(1)}, bf16[128,1408]{1,0:T(8,128)(2,1)}, u32[]{:S(2)}) copy-start(bf16[128,1408]{1,0:T(8,128)(2,1)} %param.8) | copy-start | bytes 1081348
  2.8 1.6 %copy-start = (bf16[384,2048]{1,0:T(8,128)(2,1)S(1)}, bf16[384,2048]{1,0:T(8,128)(2,1)}, u32[]{:S(2)}) copy-start(bf16[384,2048]{1,0:T(8,128)(2,1)} %x_ref.1) | copy-start | bytes 4718596
  2.8 1.6 %copy-start.5 = (f32[2048]{0:T(1024)S(1)}, f32[2048]{0:T(1024)}, u32[]{:S(2)}) copy-start(f32[2048]{0:T(1024)} %param.7) | copy-start | bytes 24580
  129.4 2.8 %copy-start.1 = (f32[1408,128]{1,0:T(8,128)S(1)}, f32[1408,128]{1,0:T(8,128)}, u32[]{:S(2)}) copy-start(f32[1408,128]{1,0:T(8,128)} %get-tuple-element.5) | copy-start | bytes 2162692
